TPU v7x, 32 devices: a whole 2x2x4 slice. The times are simulated.
32 devices in a mesh: sp: 8 (over z, x), tp: 4 (over y, core).
Axes of the slice: x: 2, y: 2, z: 4, core: 2. Of those that a mesh axis runs over, the one named last changes fastest.
Arguments:
- features: bfloat16 [3072, 2048], P('sp', 'tp'), may hold values from -6 to 6
- norm_gain: float32 [2048], replicated, may hold values from 0.28 to 10
- w_query: bfloat16 [2048, 1024], P(None, 'tp'), may hold values from -0.125 to 0.125
- w_key: bfloat16 [2048, 512], P(None, 'tp'), may hold values from -0.125 to 0.125
- w_value: bfloat16 [2048, 512], P(None, 'tp'), may hold values from -0.125 to 0.125
- head_sinks: float32 [16], P('tp'), may hold values from 1 to 5
- w_query_latent: bfloat16 [2048, 512], replicated, may hold values from -0.125 to 0.125
- w_kv_latent: bfloat16 [2048, 512], replicated, may hold values from -0.125 to 0.125
- w_rope_key: bfloat16 [2048, 64], replicated, may hold values from -0.125 to 0.125
- query_latent_gain: float32 [512], replicated, may hold values from 0.28 to 10
- kv_latent_gain: float32 [512], replicated, may hold values from 0.28 to 10
- w_query_content: bfloat16 [512, 1024], P(None, 'tp'), may hold values from -0.25 to 0.25
- w_query_rotary: bfloat16 [512, 512], P(None, 'tp'), may hold values from -0.25 to 0.25
- w_key_up: bfloat16 [512, 1024], P(None, 'tp'), may hold values from -0.25 to 0.25
- w_value_up: bfloat16 [512, 1024], P(None, 'tp'), may hold values from -0.25 to 0.25
- w_branch_window: bfloat16 [1024, 2048], P('tp'), may hold values from -0.1875 to 0.1875
- w_branch_latent: bfloat16 [1024, 2048], P('tp'), may hold values from -0.1875 to 0.1875
- w_gate_window: bfloat16 [2048, 2048], P(None, 'tp'), may hold values from -0.125 to 0.125
- w_gate_latent: bfloat16 [2048, 2048], P(None, 'tp'), may hold values from -0.125 to 0.125
Outputs:
- mixed: bfloat16 [3072, 2048], P('sp', 'tp')
All inputs are finite; a program needn't handle non-finite values.
Results may differ from a plain program's by a relative error of at most 0.018.
The roundings to bfloat16 on the way count: a program that leaves them out, or rounds other values in their place, can miss the bound.
Values may be sent and summed in bfloat16 or wider, within the bound.
A program may use at most 128 MiB of HBM per device.

v0:
```python
import jax
import jax.numpy as jnp
from jax import lax
from jax.sharding import PartitionSpec as P

HEAD = 64
WINDOW = 128
NOPE = 128
ROPE = 64
VDIM = 128


EPS = 1e-06
THETA = 10000.0
NEGATIVE = -1e30


def from_behind(shard, axis, by):
    count = lax.axis_size(axis)
    pairs = [(i, i + by) for i in range(count) if 0 <= i + by < count]
    return lax.ppermute(shard, axis, pairs)


def rms_rows(float_rows, gain_vec):
    return (
        float_rows
        * lax.rsqrt(jnp.mean(float_rows * float_rows, axis=-1, keepdims=True) + EPS)
        * gain_vec
    )


def rotate(float_rows, positions):
    half_width = float_rows.shape[-1] // 2
    frequencies = THETA ** (-jnp.arange(half_width, dtype=jnp.float32) / half_width)
    angles = positions.astype(jnp.float32)[:, None] * frequencies
    target = (float_rows.shape[0],) + (1,) * (float_rows.ndim - 2) + (half_width,)
    cosine = jnp.cos(angles).reshape(target)
    sine_part = jnp.sin(angles).reshape(target)
    first_half = float_rows[..., :half_width]
    second_half = float_rows[..., half_width:]
    return jnp.concatenate(
        [
            first_half * cosine - second_half * sine_part,
            second_half * cosine + first_half * sine_part,
        ],
        axis=-1,
    )


def project(left, right):
    return jnp.dot(left, right, preferred_element_type=jnp.float32)


def window_attention(queries, key_ext, value_ext, sink_table, row_start):
    row_count = queries.shape[0]
    kv_heads = key_ext.shape[1] // HEAD
    group_size = queries.shape[1] // HEAD // kv_heads
    blocks = row_count // WINDOW
    query_blocks = queries.reshape(blocks, WINDOW, kv_heads, group_size, HEAD)

    def banded(table):
        table = table.reshape(blocks + 1, WINDOW, kv_heads, HEAD)
        return jnp.concatenate([table[:-1], table[1:]], axis=1)

    key_band = banded(key_ext)
    value_band = banded(value_ext)
    scores = jnp.einsum(
        "nqhgd,nkhd->nhgqk", query_blocks, key_band, preferred_element_type=jnp.float32
    ) * HEAD ** (-0.5)
    query_index = jnp.arange(WINDOW, dtype=jnp.int32)[:, None]
    key_index = jnp.arange(2 * WINDOW, dtype=jnp.int32)[None, :]
    offset = query_index + WINDOW - key_index
    key_position = (
        row_start + jnp.arange(blocks, dtype=jnp.int32)[:, None, None] * WINDOW + key_index - WINDOW
    )
    valid_mask = ((offset >= 0) & (offset < WINDOW) & (key_position >= 0))[:, None, None]
    scores = jnp.where(valid_mask, scores, NEGATIVE)
    sink_logit = sink_table.reshape(1, kv_heads, group_size, 1, 1)
    row_top = jnp.maximum(jnp.max(scores, axis=-1, keepdims=True), sink_logit)
    weights = jnp.where(valid_mask, jnp.exp(scores - row_top), 0.0)
    denominator = jnp.sum(weights, axis=-1, keepdims=True) + jnp.exp(sink_logit - row_top)
    probabilities = (weights / denominator).astype(jnp.bfloat16)
    attended = jnp.einsum(
        "nhgqk,nkhd->nqhgd", probabilities, value_band, preferred_element_type=jnp.float32
    )
    return attended.astype(jnp.bfloat16).reshape(row_count, kv_heads * group_size * HEAD)


def on_device(
    features,
    norm_gain,
    w_query,
    w_key,
    w_value,
    head_sinks,
    w_query_latent,
    w_kv_latent,
    w_rope_key,
    query_latent_gain,
    kv_latent_gain,
    w_query_content,
    w_query_rotary,
    w_key_up,
    w_value_up,
    w_branch_window,
    w_branch_latent,
    w_gate_window,
    w_gate_latent,
):
    tok_rows = features.shape[0]
    row_start = lax.axis_index("sp") * tok_rows
    row_end = row_start + tok_rows
    positions = row_start + jnp.arange(tok_rows, dtype=jnp.int32)
    gathered = lax.all_gather(features, "tp", axis=1, tiled=True)
    normed = rms_rows(gathered.astype(jnp.float32), norm_gain).astype(jnp.bfloat16)
    query_rows = project(normed, w_query).astype(jnp.bfloat16)
    key_rows = project(normed, w_key).astype(jnp.bfloat16)
    value_rows = project(normed, w_value).astype(jnp.bfloat16)
    key_width = key_rows.shape[1]
    packed = jnp.concatenate([key_rows, value_rows], axis=1)
    tail_rows = from_behind(packed[tok_rows - WINDOW :], "sp", 1)
    extended = jnp.concatenate([tail_rows, packed], axis=0)
    window_out = window_attention(
        query_rows, extended[:, :key_width], extended[:, key_width:], head_sinks, row_start
    )
    latent_query = rms_rows(project(normed, w_query_latent), query_latent_gain).astype(jnp.bfloat16)
    latent_kv = rms_rows(project(normed, w_kv_latent), kv_latent_gain).astype(jnp.bfloat16)
    rope_rows = rotate(project(normed, w_rope_key), positions).astype(jnp.bfloat16)
    lat_heads = w_key_up.shape[1] // NOPE
    query_content = (
        project(latent_query, w_query_content)
        .astype(jnp.bfloat16)
        .reshape(tok_rows, lat_heads, NOPE)
    )
    query_rotary = rotate(
        project(latent_query, w_query_rotary).reshape(tok_rows, lat_heads, ROPE), positions
    ).astype(jnp.bfloat16)
    scale_factor = (NOPE + ROPE) ** (-0.5)

    def attend(running, piece_keys, piece_values, rope_piece):
        running_max, denominator, accumulated = running
        piece_rows = piece_keys.shape[0]
        scores = (
            jnp.einsum(
                "qhd,khd->hqk",
                query_content,
                piece_keys.reshape(piece_rows, lat_heads, NOPE),
                preferred_element_type=jnp.float32,
            )
            + jnp.einsum(
                "qhr,kr->hqk", query_rotary, rope_piece, preferred_element_type=jnp.float32
            )
        ) * scale_factor
        key_position = jnp.arange(piece_rows, dtype=jnp.int32)
        live_mask = key_position[None, :] <= positions[:, None]
        scores = jnp.where(live_mask, scores, NEGATIVE)
        new_max = jnp.maximum(running_max, jnp.max(scores, axis=-1))
        weights = jnp.where(live_mask, jnp.exp(scores - new_max[..., None]), 0.0)
        denominator = jnp.sum(weights, axis=-1)
        accumulated = jnp.einsum(
            "hqk,khd->hqd",
            weights.astype(jnp.bfloat16),
            piece_values.reshape(piece_rows, lat_heads, VDIM),
            preferred_element_type=jnp.float32,
        )
        return (new_max, denominator, accumulated)

    initial = (
        jnp.full((lat_heads, tok_rows), NEGATIVE, jnp.float32),
        jnp.zeros((lat_heads, tok_rows), jnp.float32),
        jnp.zeros((lat_heads, tok_rows, VDIM), jnp.float32),
    )
    pieces = (
        lax.all_gather(latent_kv, "sp", axis=0, tiled=True),
        lax.all_gather(rope_rows, "sp", axis=0, tiled=True),
    )

    def compute(current):
        piece_keys = project(pieces[0], w_key_up).astype(jnp.bfloat16)
        piece_values = project(pieces[0], w_value_up).astype(jnp.bfloat16)
        return attend(current, piece_keys, piece_values, pieces[1])

    running = lax.cond(jnp.int32(0) < row_end, compute, lambda current: current, initial)
    latent_out = jnp.transpose(running[2] / running[1][..., None], (1, 0, 2))
    latent_out = latent_out.reshape(tok_rows, lat_heads * VDIM).astype(jnp.bfloat16)
    all_window, all_latent = (
        lax.all_gather(window_out, "tp", axis=1, tiled=True),
        lax.all_gather(latent_out, "tp", axis=1, tiled=True),
    )
    column_window, column_latent = (
        lax.all_to_all(w_branch_window, "tp", split_axis=1, concat_axis=0, tiled=True),
        lax.all_to_all(w_branch_latent, "tp", split_axis=1, concat_axis=0, tiled=True),
    )
    window_branch = project(all_window, column_window)
    latent_branch = project(all_latent, column_latent)
    window_gate = jax.nn.sigmoid(project(normed, w_gate_window))
    latent_gate = jax.nn.sigmoid(project(normed, w_gate_latent))
    return (window_gate * window_branch + latent_gate * latent_branch).astype(jnp.bfloat16)


def solution(mesh):
    return jax.shard_map(
        on_device,
        mesh=mesh,
        in_specs=(
            P("sp", "tp"),
            P(),
            P(None, "tp"),
            P(None, "tp"),
            P(None, "tp"),
            P("tp"),
            P(),
            P(),
            P(),
            P(),
            P(),
            P(None, "tp"),
            P(None, "tp"),
            P(None, "tp"),
            P(None, "tp"),
            P("tp", None),
            P("tp", None),
            P(None, "tp"),
            P(None, "tp"),
        ),
        out_specs=P("sp", "tp"),
        check_vma=False,
    )
```

profile of v0, /device:TPU:0, one launch (start us, length us, event | category | flops | bytes accessed | tf_op | source)
XLA Modules:
  0.0 168.1 jit_solution(3678124389484324087)
XLA Ops:
  6.5 0.7 all-gather.3.cloned.1.call-update
  7.3 2.3 %copy.60 = bf16[256,2048]{0,1:T(8,128)(2,1)} copy(bf16[256,2048]{1,0:T(8,128)(2,1)} %param.37) | data formatting | bytes 2097152 | tf_op args[16]
  9.5 4.4 %all-to-all-start.1 = ((bf16[256,4,512]{0,2,1:T(8,128)(2,1)}), bf16[256,4,512]{0,2,1:T(8,128)(2,1)S(1)}, u32[]{:S(2)}, u32[]{:S(2)}) async-start(bf16[256,4,512]{0,2,1:T(8,128)(2,1)} %bitcast.96), calls=%async_computation.1 | async-start | bytes 2097152 | tf_op jit(solution)/shard_map/all_to_all | solution.py:192
  13.9 0.0 copy-done.26
  13.9 0.1 max.18
  14.0 2.3 %copy.57 = bf16[256,2048]{0,1:T(8,128)(2,1)} copy(bf16[256,2048]{1,0:T(8,128)(2,1)} %param.36) | data formatting | bytes 2097152 | tf_op args[15]
  16.3 19.8 %all-to-all-done.1 = bf16[256,4,512]{0,2,1:T(8,128)(2,1)S(1)} async-done(((bf16[256,4,512]{0,2,1:T(8,128)(2,1)}), bf16[256,4,512]{0,2,1:T(8,128)(2,1)S(1)}, u32[]{:S(2)}, u32[]{:S(2)}) %all-to-all-start.1) | async-done | bytes 1048608 | tf_op jit(solution)/shard_map/all_to_all | solution.py:192
  36.1 4.2 %all-to-all-start = ((bf16[256,4,512]{0,2,1:T(8,128)(2,1)}), bf16[256,4,512]{0,2,1:T(8,128)(2,1)}, u32[]{:S(2)}, u32[]{:S(2)}) async-start(bf16[256,4,512]{0,2,1:T(8,128)(2,1)} %bitcast.97), calls=%async_computation | async-start | bytes 2097152 | tf_op jit(solution)/shard_map/all_to_all | solution.py:191
  40.3 0.0 all-gather.5.cloned.1.call-start
  40.4 0.1 add_compare_fusion
  40.5 0.2 broadcast_and_fusion
  40.7 1.3 copy.61
  42.0 12.8 %all-to-all-done = bf16[256,4,512]{0,2,1:T(8,128)(2,1)} async-done(((bf16[256,4,512]{0,2,1:T(8,128)(2,1)}), bf16[256,4,512]{0,2,1:T(8,128)(2,1)}, u32[]{:S(2)}, u32[]{:S(2)}) %all-to-all-start) | async-done | bytes 1048608 | tf_op jit(solution)/shard_map/all_to_all | solution.py:191
  54.8 2.3 %copy.58 = bf16[4,256,512]{2,1,0:T(8,128)(2,1)} copy(bf16[4,256,512]{1,2,0:T(8,128)(2,1)} %bitcast.12) | data formatting | bytes 2097152 | tf_op jit(solution)/shard_map/all_to_all | solution.py:191
  57.1 1.9 %fusion.14 = f32[384]{0:T(512)S(1)} fusion(bf16[384,2048]{1,0:T(8,128)(2,1)} %all-gather.3.cloned.1.call-done), kind=kLoop, calls=%fused_computation.22 | loop fusion | flops 2358912 | bytes 1574400 | tf_op jit(solution)/shard_map/reduce_sum | solution.py:27
  59.1 0.4 fusion.16
  59.5 0.0 copy-done
  59.5 0.0 copy-start.23
  59.5 1.1 multiply_reduce_fusion.1
  60.6 0.1 copy-done.2
  60.7 0.9 multiply_convert_fusion.1
  61.6 0.0 all-gather.5.cloned.1.call-update
  61.6 0.1 copy-done.12
  61.7 2.0 %convolution_convert_fusion.6 = bf16[384,128]{0,1:T(8,128)(2,1)S(1)} fusion(bf16[384,2048]{1,0:T(8,128)(2,1)} %copy-done.2, bf16[2048,128]{1,0:T(8,128)(2,1)S(1)} %copy-done.12), kind=kOutput, calls=%fused_computation.46 | convolution fusion | flops 201375744 | bytes 2195456 | tf_op jit(solution)/shard_map/dot_general | solution.py:51
  63.8 2.0 %convolution_convert_fusion.5 = bf16[384,128]{0,1:T(8,128)(2,1)S(1)} fusion(bf16[384,2048]{1,0:T(8,128)(2,1)} %copy-done.2, bf16[2048,128]{1,0:T(8,128)(2,1)S(1)} %copy-done.13), kind=kOutput, calls=%fused_computation.45 | convolution fusion | flops 201375744 | bytes 2195456 | tf_op jit(solution)/shard_map/dot_general | solution.py:51
  65.8 0.6 pad_maximum_fusion.4
  66.5 5.2 %collective-permute-start = (bf16[128,256]{0,1:T(8,128)(2,1)}, bf16[128,256]{0,1:T(8,128)(2,1)}, u32[]{:S(2)}, u32[]{:S(2)}) collective-permute-start(bf16[128,256]{0,1:T(8,128)(2,1)} %pad_maximum_fusion.4), channel_id=1, source_target_pairs={{0,4},{4,8},{8,12},{12,16},{16,20},{20,24},{24,28},{1,5},{5,9},{9,... | collective-permute-start | bytes 196616 | tf_op jit(solution)/shard_map/ppermute | solution.py:21
  71.7 0.6 copy.52
  72.3 2.3 %convolution_convert_fusion.3 = bf16[384,256]{1,0:T(8,128)(2,1)S(1)} fusion(bf16[384,2048]{1,0:T(8,128)(2,1)} %copy-done.2, bf16[2048,256]{1,0:T(8,128)(2,1)} %param.23), kind=kOutput, calls=%fused_computation.42 | convolution fusion | flops 402751488 | bytes 2818048 | tf_op jit(solution)/shard_map/dot_general | solution.py:51
  74.7 0.2 reshape.210
  74.9 2.1 %fusion.41 = f32[384,64]{0,1:T(8,128)S(1)} fusion(bf16[384,2048]{1,0:T(8,128)(2,1)} %copy-done.2, bf16[2048,64]{0,1:T(8,128)(2,1)S(1)} %copy-done.18), kind=kOutput, calls=%fused_computation.93 | convolution fusion | flops 100663296 | bytes 1933312 | tf_op jit(solution)/shard_map/dot_general | solution.py:51
  77.0 0.3 multiply_cosine_fusion
  77.3 35.1 %all_gather.18 = bf16[3072,64]{0,1:T(8,128)(2,1)} all-gather(bf16[384,64]{0,1:T(8,128)(2,1)S(1)} %pad_maximum_fusion.5), channel_id=1, replica_groups=mesh['sp'=8,'tp'=4] {'sp'}, dimensions={0}, use_global_device_ids=true | all-gather | bytes 442368 | tf_op jit(solution)/shard_map/all_gather | solution.py:175
  112.5 2.7 %multiply_reduce_fusion = (f32[384]{0:T(512)S(1)}, f32[384,512]{1,0:T(8,128)S(1)}) fusion(bf16[384,2048]{1,0:T(8,128)(2,1)S(1)} %copy-done.3, bf16[2048,512]{1,0:T(8,128)(2,1)} %param.27), kind=kOutput, calls=%fused_computation.48 | convolution fusion | flops 805699200 | bytes 4457984 | tf_op jit(solution)/shard_map/dot_general | solution.py:51
  115.1 0.0 copy-start.24
  115.2 0.4 fusion.38
  115.6 0.5 copy-done.15
  116.1 1.0 convolution_convert_fusion.2
  117.1 2.0 %fusion.24 = f32[384,512]{1,0:T(8,128)} fusion(bf16[384,2048]{1,0:T(8,128)(2,1)S(1)} %copy-done.3, bf16[2048,512]{1,0:T(8,128)(2,1)S(1)} %copy-done.24), kind=kOutput, calls=%fused_computation.39 | convolution fusion | flops 805896192 | bytes 4456448 | tf_op jit(solution)/shard_map/dot_general | solution.py:51
  119.1 2.0 %fusion.22 = f32[384,512]{1,0:T(8,128)} fusion(bf16[384,2048]{1,0:T(8,128)(2,1)S(1)} %copy-done.3, bf16[2048,512]{1,0:T(8,128)(2,1)S(1)} %copy-done.25), kind=kOutput, calls=%fused_computation.37 | convolution fusion | flops 805896192 | bytes 4456448 | tf_op jit(solution)/shard_map/dot_general | solution.py:51
  121.0 0.6 pad_maximum_fusion.3
  121.7 0.0 collective-permute-done
  121.7 0.8 pad_maximum_fusion.2
  122.6 0.4 fusion.40
  123.1 0.1 broadcast_maximum_fusion.1
  123.1 0.3 fusion.20
  123.5 0.1 exponential_add_fusion
  123.5 0.5 fusion.26
  124.0 0.2 copy.56
  124.3 7.9 %all_gather.16 = bf16[384,1024]{0,1:T(8,128)(2,1)} all-gather(bf16[384,256]{0,1:T(8,128)(2,1)S(1)} %bitcast.100), channel_id=1, replica_groups=mesh['sp'=8,'tp'=4] {'tp'}, dimensions={1}, use_global_device_ids=true | all-gather | bytes 983040 | tf_op jit(solution)/shard_map/all_gather | solution.py:187
  132.2 15.7 %conditional.1 = (f32[2,384]{1,0:T(2,128)S(1)}, f32[2,384,128]{1,2,0:T(8,128)}) conditional(s32[]{:T(128)} %convert_element_type.75, () %tuple.13, (s32[]{:T(128)}, s32[384]{0:T(512)S(1)}, bf16[3072,512]{1,0:T(8,128)(2,1)}, bf16[512,256]{1,0:T(8,128)(2,1)S(1)}, bf16[384,256]{1,0:T(8,128)(2,1)}, /*index=5*/bf16[3072,64]{0,1:T(8,128)(2,1)}, ...), branch_computations={%region_5.6_spmd, %region_6.9_spmd} | conditional | flops 3146907136 | bytes 87218872 | solution.py:183
  132.2 0.9 iota_compare_fusion
  133.1 3.4 %convolution_convert_fusion.1 = bf16[3072,256]{0,1:T(8,128)(2,1)S(1)} fusion(bf16[3072,512]{1,0:T(8,128)(2,1)} %get-tuple-element.26, bf16[512,256]{1,0:T(8,128)(2,1)S(1)} %get-tuple-element.38), kind=kOutput, calls=%fused_computation.12 | convolution fusion | flops 806092800 | bytes 4980736 | tf_op jit(solution)/shard_map/cond/branch_1_fun/dot_general | solution.py:51
  136.5 1.6 fusion.10
  138.1 0.0 copy-start.17
  138.1 2.4 %fusion.39 = (f32[2,384]{1,0:T(2,128)S(1)}, f32[2,384,3072]{1,2,0:T(8,128)S(1)}) fusion(bf16[384,2,64]{0,2,1:T(8,128)(2,1)S(1)} %copy-done.14, bf16[3072,64]{0,1:T(8,128)(2,1)S(1)} %copy-done.9, f32[2,3072,384]{2,1,0:T(8,128)S(1)} %fusion.10, pred[384,3072]{0,1:T(8,128)(4,1)S(1)} %iota_compare_fusion), kind=kOutput, calls=%fused_computation.91 | convolution fusion | flops 311426304 | bytes 20548608 | tf_op jit(solution)/shard_map/cond/branch_1_fun/qhr,kr->hqk/dot_general | solution.py:150
  140.5 1.0 convolution_convert_fusion
  141.6 3.1 %fusion.4 = f32[2,384,128]{1,2,0:T(8,128)} fusion(bf16[3072,2,128]{0,2,1:T(8,128)(2,1)S(1)} %bitcast.93, f32[2,384,3072]{1,2,0:T(8,128)S(1)} %get-tuple-element.42, f32[2,384]{1,0:T(2,128)S(1)} %broadcast_maximum_fusion, pred[384,3072]{0,1:T(8,128)(4,1)S(1)} %iota_compare_fusion), kind=kOutput, calls=%fused_computation.6 | convolution fusion | flops 611057664 | bytes 12585984 | tf_op jit(solution)/shard_map/cond | solution.py:183
  144.7 3.2 %fusion.3 = f32[2,384]{1,0:T(2,128)S(1)} fusion(f32[2,384,3072]{1,2,0:T(8,128)S(1)} %get-tuple-element.42, f32[2,384]{1,0:T(2,128)S(1)} %broadcast_maximum_fusion, pred[384,3072]{0,1:T(8,128)(4,1)} %copy-done.4), kind=kLoop, calls=%fused_computation.5 | loop fusion | flops 7077120 | bytes 10622976 | tf_op jit(solution)/shard_map/cond/branch_1_fun/reduce_sum | solution.py:159
  147.9 1.1 divide_convert_fusion.2
  149.0 9.0 %all_gather.19 = bf16[384,1024]{0,1:T(8,128)(2,1)S(1)} all-gather(bf16[384,256]{0,1:T(8,128)(2,1)S(1)} %bitcast.102), channel_id=1, replica_groups=mesh['sp'=8,'tp'=4] {'tp'}, dimensions={1}, use_global_device_ids=true | all-gather | bytes 983040 | tf_op jit(solution)/shard_map/all_gather | solution.py:188
  158.0 1.9 %convolution_multiply_fusion = f32[384,512]{1,0:T(8,128)S(1)} fusion(f32[384,512]{1,0:T(8,128)} %fusion.24, bf16[384,1024]{0,1:T(8,128)(2,1)S(1)} %all_gather.19, bf16[1024,512]{1,0:T(8,128)(2,1)S(1)} %bitcast.94), kind=kOutput, calls=%fused_computation.28 | convolution fusion | flops 402849792 | bytes 3407872 | tf_op jit(solution)/shard_map/dot_general | solution.py:51
  159.9 0.0 copy-done.10
  159.9 1.4 fusion.25
  (69 shorter events, 0.4 us)
Async XLA Ops:
  6.5 53.0 %copy-start = (bf16[2048,512]{1,0:T(8,128)(2,1)S(1)}, bf16[2048,512]{1,0:T(8,128)(2,1)}, u32[]{:S(2)}) copy-start(bf16[2048,512]{1,0:T(8,128)(2,1)} %param.28) | copy-start | bytes 6291460
  6.5 50.6 %all-gather.3.cloned.1.call-start = ((), (), s32[]{:S(2)}) async-start(), calls=%async_computation.2 | async-start | bytes 1966080 | tf_op jit(solution)/shard_map/all_gather | solution.py:114
  9.5 4.4 %copy-start.26 = (f32[4]{0:T(128)S(1)}, f32[4]{0:T(128)}, u32[]{:S(2)}) copy-start(f32[4]{0:T(128)} %param.26) | copy-start | bytes 52
  9.5 26.6 %all-to-all-start.1 = ((bf16[256,4,512]{0,2,1:T(8,128)(2,1)}), bf16[256,4,512]{0,2,1:T(8,128)(2,1)S(1)}, u32[]{:S(2)}, u32[]{:S(2)}) async-start(bf16[256,4,512]{0,2,1:T(8,128)(2,1)} %bitcast.96), calls=%async_computation.1 | async-start | bytes 2097152 | tf_op jit(solution)/shard_map/all_to_all | solution.py:192
  36.1 18.7 %all-to-all-start = ((bf16[256,4,512]{0,2,1:T(8,128)(2,1)}), bf16[256,4,512]{0,2,1:T(8,128)(2,1)}, u32[]{:S(2)}, u32[]{:S(2)}) async-start(bf16[256,4,512]{0,2,1:T(8,128)(2,1)} %bitcast.97), calls=%async_computation | async-start | bytes 2097152 | tf_op jit(solution)/shard_map/all_to_all | solution.py:191
  40.3 91.8 %all-gather.5.cloned.1.call-start = ((), (), s32[]{:S(2)}) async-start(), calls=%async_computation.3 | async-start | bytes 3538944 | tf_op jit(solution)/shard_map/all_gather | solution.py:174
  54.8 4.2 %copy-start.21 = (f32[2048]{0:T(1024)S(1)}, f32[2048]{0:T(1024)}, u32[]{:S(2)}) copy-start(f32[2048]{0:T(1024)} %param.22) | copy-start | bytes 24580
  57.1 1.9 %copy-start.5 = (bf16[384,2048]{1,0:T(8,128)(2,1)S(1)}, bf16[384,2048]{1,0:T(8,128)(2,1)}, u32[]{:S(2)}) copy-start(bf16[384,2048]{1,0:T(8,128)(2,1)} %all-gather.3.cloned.1.call-done) | copy-start | bytes 4718596
  59.5 1.2 copy-start.2
  59.5 1.2 copy-start.23
  60.7 1.0 copy-start.12
  61.6 2.2 %copy-start.13 = (bf16[2048,128]{1,0:T(8,128)(2,1)S(1)}, bf16[2048,128]{1,0:T(8,128)(2,1)}, u32[]{:S(2)}) copy-start(bf16[2048,128]{1,0:T(8,128)(2,1)} %param.25) | copy-start | bytes 1572868
  66.5 55.2 %collective-permute-start = (bf16[128,256]{0,1:T(8,128)(2,1)}, bf16[128,256]{0,1:T(8,128)(2,1)}, u32[]{:S(2)}, u32[]{:S(2)}) collective-permute-start(bf16[128,256]{0,1:T(8,128)(2,1)} %pad_maximum_fusion.4), channel_id=1, source_target_pairs={{0,4},{4,8},{8,12},{12,16},{16,20},{20,24},{24,28},{1,5},{5,9},{9,... | collective-permute-start | bytes 196616 | tf_op jit(solution)/shard_map/ppermute | solution.py:21
  72.3 2.6 %copy-start.18 = (bf16[2048,64]{0,1:T(8,128)(2,1)S(1)}, bf16[2048,64]{0,1:T(8,128)(2,1)}, u32[]{:S(2)}) copy-start(bf16[2048,64]{0,1:T(8,128)(2,1)} %param.29) | copy-start | bytes 786436
  74.9 37.6 %copy-start.3 = (bf16[384,2048]{1,0:T(8,128)(2,1)S(1)}, bf16[384,2048]{1,0:T(8,128)(2,1)}, u32[]{:S(2)}) copy-start(bf16[384,2048]{1,0:T(8,128)(2,1)} %copy-done.2) | copy-start | bytes 4718596
  112.4 2.7 %copy-start.19 = (bf16[512,128]{1,0:T(8,128)(2,1)S(1)}, bf16[512,128]{1,0:T(8,128)(2,1)}, u32[]{:S(2)}) copy-start(bf16[512,128]{1,0:T(8,128)(2,1)} %param.33) | copy-start | bytes 393220
  112.4 2.7 %copy-start.22 = (f32[512]{0:T(512)S(1)}, f32[512]{0:T(512)}, u32[]{:S(2)}) copy-start(f32[512]{0:T(512)} %param.30) | copy-start | bytes 6148
  115.1 1.0 copy-start.15
  115.1 1.9 %copy-start.24 = (bf16[2048,512]{1,0:T(8,128)(2,1)S(1)}, bf16[2048,512]{1,0:T(8,128)(2,1)}, u32[]{:S(2)}) copy-start(bf16[2048,512]{1,0:T(8,128)(2,1)} %param.39) | copy-start | bytes 6291460
  117.1 2.0 %copy-start.25 = (bf16[2048,512]{1,0:T(8,128)(2,1)S(1)}, bf16[2048,512]{1,0:T(8,128)(2,1)}, u32[]{:S(2)}) copy-start(bf16[2048,512]{1,0:T(8,128)(2,1)} %param.38) | copy-start | bytes 6291460
  121.0 1.6 copy-start.20
  124.0 8.1 %copy-start.16 = (bf16[512,256]{1,0:T(8,128)(2,1)S(1)}, bf16[512,256]{1,0:T(8,128)(2,1)}, u32[]{:S(2)}) copy-start(bf16[512,256]{1,0:T(8,128)(2,1)} %param.34) | copy-start | bytes 786436
  133.1 8.5 %copy-start.4 = (pred[384,3072]{0,1:T(8,128)(4,1)}, pred[384,3072]{0,1:T(8,128)(4,1)S(1)}, u32[]{:S(2)}) copy-start(pred[384,3072]{0,1:T(8,128)(4,1)S(1)} %iota_compare_fusion) | copy-start | bytes 3538948 | tf_op jit(solution)/shard_map/cond
  133.1 3.4 %copy-start.11 = (bf16[384,256]{1,0:T(8,128)(2,1)S(1)}, bf16[384,256]{1,0:T(8,128)(2,1)}, u32[]{:S(2)}) copy-start(bf16[384,256]{1,0:T(8,128)(2,1)} %get-tuple-element.28) | copy-start | bytes 589828 | tf_op jit(solution)/shard_map/cond
  136.5 1.6 copy-start.9
  136.5 1.6 copy-start.14
  138.1 2.5 %copy-start.1 = (bf16[3072,512]{1,0:T(8,128)(2,1)S(1)}, bf16[3072,512]{1,0:T(8,128)(2,1)}, u32[]{:S(2)}) copy-start(bf16[3072,512]{1,0:T(8,128)(2,1)} %get-tuple-element.26) | copy-start | bytes 9437188 | tf_op jit(solution)/shard_map/cond
  138.1 2.5 %copy-start.17 = (bf16[512,256]{1,0:T(8,128)(2,1)S(1)}, bf16[512,256]{1,0:T(8,128)(2,1)}, u32[]{:S(2)}) copy-start(bf16[512,256]{1,0:T(8,128)(2,1)} %get-tuple-element.39) | copy-start | bytes 786436 | tf_op jit(solution)/shard_map/cond
  147.9 10.1 %copy-start.6 = (bf16[4,256,512]{2,1,0:T(8,128)(2,1)S(1)}, bf16[4,256,512]{2,1,0:T(8,128)(2,1)}, u32[]{:S(2)}) copy-start(bf16[4,256,512]{2,1,0:T(8,128)(2,1)} %copy.61) | copy-start | bytes 3145732
  158.0 1.9 %copy-start.7 = (bf16[4,256,512]{2,1,0:T(8,128)(2,1)S(1)}, bf16[4,256,512]{2,1,0:T(8,128)(2,1)}, u32[]{:S(2)}) copy-start(bf16[4,256,512]{2,1,0:T(8,128)(2,1)} %copy.58) | copy-start | bytes 3145732
  158.0 1.9 %copy-start.8 = (bf16[384,1024]{0,1:T(8,128)(2,1)S(1)}, bf16[384,1024]{0,1:T(8,128)(2,1)}, u32[]{:S(2)}) copy-start(bf16[384,1024]{0,1:T(8,128)(2,1)} %all_gather.16) | copy-start | bytes 2359300
  158.0 1.9 %copy-start.10 = (f32[384,512]{1,0:T(8,128)S(1)}, f32[384,512]{1,0:T(8,128)}, u32[]{:S(2)}) copy-start(f32[384,512]{1,0:T(8,128)} %fusion.22) | copy-start | bytes 2359300
Sparse Core Ops, SparseCore 0:
  8.9 29.3 all-gather.2
  61.7 65.5 all-gather.4
where the time goes:
time: 169 us; the launch traced here: 168 us
  blocking collectives  52 us (31%)
  waiting for transfers between devices  33.3 us (20%)
  matrix products  33.2 us (20%)
  starting transfers between devices  13.9 us (8%)
  between operations  13.7 us (8%)
  other arithmetic  11.6 us (7%)
  local copies, waits for them, and re-layouts  10.3 us (6%)
    all_gather x1, blocking collectives, on_device(): lax.all_gather(rope_rows, 'sp', axis=0, tiled=True)  35.1 us
    dot_general x14, matrix products, project(): return jnp.dot(left, right, preferred_element_type=jnp.float32)  25.1 us
    all_to_all x1, waiting for transfers between devices, on_device(): lax.all_to_all(w_branch_latent, 'tp', split_axis=1, concat_axis=0, tiled=...  19.8 us
    all_to_all x1, waiting for transfers between devices, on_device(): lax.all_to_all(w_branch_window, 'tp', split_axis=1, concat_axis=0, tiled=...  12.8 us
    all_gather x1, blocking collectives, on_device(): lax.all_gather(latent_out, 'tp', axis=1, tiled=True)  8.98 us
    all_gather x1, blocking collectives, on_device(): lax.all_gather(window_out, 'tp', axis=1, tiled=True)  7.89 us
    unnamed x45, local copies, waits for them, and re-layouts  5.36 us
    ppermute x1, starting transfers between devices, from_behind(): return lax.ppermute(shard, axis, pairs)  5.23 us
  transfers between devices with their start and end apart: 5, of which 2 were waited for; matrix products, arithmetic and copies ran while one was open for 18% of the time, Pallas kernels for 0%

commit v1 on v0

v1 whole, which is shorter than its diff:
```python
import functools

import jax
import jax.numpy as jnp
from jax import lax
from jax.experimental import pallas as pl
from jax.experimental.pallas import tpu as pltpu
from jax.sharding import PartitionSpec as P

HEAD = 64
WINDOW = 128
NOPE = 128
ROPE = 64
VDIM = 128


EPS = 1e-06
THETA = 10000.0
NEGATIVE = -1e30
LANES = 128
MESH = pl.DeviceIdType.MESH
BF16 = jnp.bfloat16
F32 = jnp.float32


def dot(left, right):
    return jnp.dot(left, right, preferred_element_type=F32)


def dot_t(left, right):
    return lax.dot_general(left, right, (((1,), (1,)), ((), ())), preferred_element_type=F32)


def rms_rows(rows, gain):
    return rows * lax.rsqrt(jnp.mean(rows * rows, axis=-1, keepdims=True) + EPS) * gain


def swap_halves(rows):
    half = rows.shape[1] // 2
    return jnp.concatenate([rows[:, half:], rows[:, :half]], axis=1)


WEIGHTS = (
    "kv_latent", "rope", "key", "value", "query", "query_latent", "content", "rotary",
    "key_up", "value_up", "gate_window", "gate_latent",
)


def kernel(dims, *refs):
    n_sp, n_tp, n_x = dims
    n_z, n_y = n_sp // n_x, n_tp // 2
    features, norm_gain, sinks, q_gain, kv_gain, cosine, sine = refs[:7]
    w_hbm = dict(zip(WEIGHTS, refs[7:19]))
    branch_hbm = refs[19:21]
    out = refs[21]
    feat, normed, wide = refs[22:25]
    w = dict(zip(WEIGHTS, refs[25:37]))
    columns = refs[37:39]
    kvb, local_kv, halo, queries, q_full, gates, win, lat, top, total, acc = refs[39:50]
    w_sem, own_sem, col_own, col_send, col_recv, halo_sem, y_send, y_recv, s_send, s_recv = refs[50:60]
    z_send, z_recv, x_send, x_recv, c_send, c_recv, d_send, d_recv = refs[60:68]

    sp, tp = lax.axis_index("sp"), lax.axis_index("tp")
    z, x = sp // n_x, lax.rem(sp, n_x)
    y, core = tp // 2, lax.rem(tp, 2)
    sibling = y * 2 + (1 - core)
    rows, block = features.shape
    half = rows // 2
    lat_heads = w_hbm["key_up"].shape[1] // NOPE
    kv_width = w_hbm["key"].shape[1]
    kv_heads = kv_width // HEAD
    group = w_hbm["query"].shape[1] // kv_width
    latent = w_hbm["kv_latent"].shape[1]

    loads = {}
    own_feat = pltpu.make_async_copy(features, feat.at[tp], own_sem.at[0])
    own_feat.start()
    for i, name in enumerate(WEIGHTS):
        loads[name] = pltpu.make_async_copy(w_hbm[name], w[name], w_sem.at[i])
        loads[name].start()

    def remote(src, dst, send, recv, where):
        return pltpu.make_async_remote_copy(
            src_ref=src, dst_ref=dst, send_sem=send, recv_sem=recv,
            device_id=where, device_id_type=MESH,
        )

    barrier = pltpu.get_barrier_semaphore()

    def greet(where):
        pl.semaphore_signal(barrier, inc=1, device_id=where, device_id_type=MESH)

    for d in range(1, n_tp):
        greet({"sp": sp, "tp": lax.rem(tp + d, n_tp)})
    for d in range(1, n_x):
        greet({"sp": z * n_x + lax.rem(x + d, n_x), "tp": tp})

    @pl.when(z + 1 < n_z)
    def _():
        greet({"sp": sp + n_x, "tp": tp})

    @pl.when(z > 0)
    def _():
        greet({"sp": sp - n_x, "tp": tp})

    @pl.when(sp + 1 < n_sp)
    def _():
        greet({"sp": sp + 1, "tp": tp})

    @pl.when(sp > 0)
    def _():
        greet({"sp": sp - 1, "tp": tp})

    one, none = jnp.int32(1), jnp.int32(0)
    pl.semaphore_wait(
        barrier,
        n_tp - 1 + n_x - 1
        + jnp.where(z + 1 < n_z, one, none) + jnp.where(z > 0, one, none)
        + jnp.where(sp + 1 < n_sp, one, none) + jnp.where(sp > 0, one, none),
    )

    def gather(buf, which):
        own = buf.at[tp]
        sends = [
            remote(own, own, y_send.at[which, d], y_recv.at[which, d],
                   {"sp": sp, "tp": lax.rem(y + d, n_y) * 2 + core})
            for d in range(1, n_y)
        ]
        sends.append(remote(own, own, s_send.at[which, 0], s_recv.at[which, 0],
                            {"sp": sp, "tp": sibling}))
        return sends

    def start(copies):
        for copy in copies:
            copy.start()

    def arrived(buf, which):
        for d in range(1, n_y):
            slot = lax.rem(y + n_y - d, n_y) * 2 + core
            ref = buf.at[slot]
            remote(ref, ref, y_send.at[which, d], y_recv.at[which, d],
                   {"sp": sp, "tp": sibling}).wait_recv()
            remote(ref, ref, s_send.at[which, d], s_recv.at[which, d],
                   {"sp": sp, "tp": sibling}).start()
        for d in range(n_y):
            ref = buf.at[lax.rem(y + n_y - d, n_y) * 2 + (1 - core)]
            remote(ref, ref, s_send.at[which, d], s_recv.at[which, d],
                   {"sp": sp, "tp": sibling}).wait_recv()

    def sent(buf, which):
        own = buf.at[tp]
        for d in range(1, n_y):
            remote(own, own, y_send.at[which, d], y_recv.at[which, d],
                   {"sp": sp, "tp": sibling}).wait_send()
        for d in range(n_y):
            remote(own, own, s_send.at[which, d], s_recv.at[which, d],
                   {"sp": sp, "tp": sibling}).wait_send()

    own_feat.wait()
    start(gather(feat, 0))
    arrived(feat, 0)

    def column_copies():
        local, sends = [], []
        for b in range(2):
            span = branch_hbm[b]
            local.append(pltpu.make_async_copy(
                span.at[:, pl.ds(pl.multiple_of(tp * block, LANES), block)],
                columns[b].at[tp], col_own.at[b]))
            for d in range(1, n_tp):
                to = lax.rem(tp + d, n_tp)
                sends.append(remote(
                    span.at[:, pl.ds(pl.multiple_of(to * block, LANES), block)],
                    columns[b].at[tp], col_send.at[b, d], col_recv.at[b, d],
                    {"sp": sp, "tp": to}))
        return local, sends

    column_local, column_sends = column_copies()
    start(column_local)
    start(column_sends)

    squares = jnp.zeros((rows, 1), F32)
    for j in range(n_tp):
        piece = feat[j].astype(F32)
        squares = squares + jnp.sum(piece * piece, axis=-1, keepdims=True)
    scale = lax.rsqrt(squares / (n_tp * block) + EPS)
    for j in range(n_tp):
        span = slice(j * block, (j + 1) * block)
        normed[:, span] = (feat[j].astype(F32) * scale * norm_gain[:, span]).astype(BF16)

    def wide_dot(name):
        loads[name].wait()
        tile = min(256, latent)

        def step(i, _):
            at = pl.ds(pl.multiple_of(i * tile, LANES), tile)
            wide[:, at] = dot(normed[...], w[name][:, at])
            return 0

        lax.fori_loop(0, w[name].shape[1] // tile, step, 0)

    wide_dot("kv_latent")
    latents = rms_rows(wide[...], kv_gain[...]).astype(BF16)
    loads["rope"].wait()
    rope = dot(normed[...], w["rope"][...])
    rope = rope * cosine[...] + swap_halves(rope) * sine[...]
    padding = jnp.zeros((rows, LANES - ROPE), F32)
    rope = jnp.concatenate([rope, padding], axis=1).astype(BF16)
    kvb[sp, :, :, :latent] = latents.reshape(2, half, latent)
    kvb[sp, :, :, latent:] = rope.reshape(2, half, LANES)

    def column_slot(k):
        return (z - k) * n_x + x

    def z_copy(k):
        ref = kvb.at[column_slot(k), core]
        return remote(ref, ref, z_send.at[k], z_recv.at[k + 1], {"sp": sp + n_x, "tp": tp})

    def x_copy(k, d):
        ref = kvb.at[column_slot(k), core]
        return remote(ref, ref, x_send.at[k, d], x_recv.at[k, d],
                      {"sp": z * n_x + lax.rem(x + d, n_x), "tp": tp})

    def c_copy(k, which):
        ref = kvb.at[column_slot(k), which]
        return remote(ref, ref, c_send.at[k], c_recv.at[k], {"sp": sp, "tp": sibling})

    def row_slot(k, d):
        return (z - k) * n_x + lax.rem(x + n_x - d, n_x)

    def d_copy(k, d, which):
        ref = kvb.at[row_slot(k, d), which]
        return remote(ref, ref, d_send.at[k, d], d_recv.at[k, d], {"sp": sp, "tp": sibling})

    def pass_on(k):
        @pl.when(z + 1 < n_z)
        def _():
            z_copy(k).start()

        for d in range(1, n_x):
            x_copy(k, d).start()

    def take_column(k):
        ref = kvb.at[column_slot(k), core]
        remote(ref, ref, z_send.at[k], z_recv.at[k], {"sp": sp, "tp": sibling}).wait_recv()
        pass_on(k)
        c_copy(k, core).start()

    def take_rows(k):
        for d in range(1, n_x):
            ref = kvb.at[row_slot(k, d), core]
            remote(ref, ref, x_send.at[k, d], x_recv.at[k, d],
                   {"sp": sp, "tp": sibling}).wait_recv()
            d_copy(k, d, core).start()

    pass_on(0)

    loads["key"].wait()
    loads["value"].wait()
    local_kv[:, :kv_width] = dot(normed[...], w["key"][...]).astype(BF16)
    local_kv[:, kv_width:] = dot(normed[...], w["value"][...]).astype(BF16)
    tail = local_kv.at[pl.ds(rows - WINDOW, WINDOW)]
    halo_copy = remote(tail, halo, halo_sem.at[0], halo_sem.at[1], {"sp": sp + 1, "tp": tp})

    @pl.when(sp + 1 < n_sp)
    def _():
        halo_copy.start()

    loads["query"].wait()
    queries[...] = dot(normed[...], w["query"][...]).astype(BF16)

    wide_dot("query_latent")
    latent_query = rms_rows(wide[...], q_gain[...]).astype(BF16)
    loads["content"].wait()
    loads["rotary"].wait()
    content = dot(latent_query, w["content"][...]).astype(BF16)
    rotary = dot(latent_query, w["rotary"][...])
    for h in range(lat_heads):
        turned = rotary[:, h * ROPE : (h + 1) * ROPE]
        turned = turned * cosine[...] + swap_halves(turned) * sine[...]
        q_full[h, :, :NOPE] = content[:, h * NOPE : (h + 1) * NOPE]
        q_full[h, :, NOPE:] = jnp.concatenate([turned, padding], axis=1).astype(BF16)
    loads["key_up"].wait()
    loads["value_up"].wait()

    def attend(slot, diagonal):
        both = kvb[slot].reshape(rows, latent + LANES)
        source, rope_part = both[:, :latent], both[:, latent:]
        keys = dot(source, w["key_up"][...]).astype(BF16)
        values = dot(source, w["value_up"][...]).astype(BF16)
        for h in range(lat_heads):
            key = jnp.concatenate([keys[:, h * NOPE : (h + 1) * NOPE], rope_part], axis=1)
            scores = dot_t(q_full[h], key) * (NOPE + ROPE) ** (-0.5)
            if diagonal:
                live = (lax.broadcasted_iota(jnp.int32, scores.shape, 1)
                        <= lax.broadcasted_iota(jnp.int32, scores.shape, 0))
                scores = jnp.where(live, scores, NEGATIVE)
            peak = jnp.max(scores, axis=-1, keepdims=True)
            if not diagonal:
                before = top[h][:, :1]
                peak = jnp.maximum(peak, before)
                fade = jnp.exp(before - peak)
            weights = jnp.exp(scores - peak)
            weight_sum = jnp.sum(weights, axis=-1, keepdims=True)
            part = dot(weights.astype(BF16), values[:, h * VDIM : (h + 1) * VDIM])
            if not diagonal:
                weight_sum = total[h][:, :1] * fade + weight_sum
                part = acc[h] * fade + part
            top[h] = jnp.broadcast_to(peak, (rows, LANES))
            total[h] = jnp.broadcast_to(weight_sum, (rows, LANES))
            acc[h] = part

    def window():
        @pl.when(sp > 0)
        def _():
            remote(tail, halo, halo_sem.at[0], halo_sem.at[1],
                   {"sp": sp, "tp": sibling}).wait_recv()

        @pl.when(sp == 0)
        def _():
            halo[...] = jnp.zeros(halo.shape, BF16)

        row = lax.broadcasted_iota(jnp.int32, (WINDOW, 2 * WINDOW), 0)
        column = lax.broadcasted_iota(jnp.int32, (WINDOW, 2 * WINDOW), 1)
        offset = row + WINDOW - column
        in_band = (offset >= 0) & (offset < WINDOW)
        for n in range(rows // WINDOW):
            at = slice(n * WINDOW, (n + 1) * WINDOW)
            earlier = halo[...] if n == 0 else local_kv[(n - 1) * WINDOW : n * WINDOW]
            band = jnp.concatenate([earlier, local_kv[at]], axis=0)
            valid = in_band & (sp * rows + n * WINDOW + column - WINDOW >= 0)
            heads = []
            for g in range(kv_heads):
                key = band[:, g * HEAD : (g + 1) * HEAD]
                value = band[:, kv_width + g * HEAD : kv_width + (g + 1) * HEAD]
                for i in range(group):
                    q = g * group + i
                    scores = dot_t(queries[at, q * HEAD : (q + 1) * HEAD], key) * HEAD ** (-0.5)
                    scores = jnp.where(valid, scores, NEGATIVE)
                    sink = sinks[0, q]
                    peak = jnp.maximum(jnp.max(scores, axis=-1, keepdims=True), sink)
                    weights = jnp.exp(scores - peak)
                    bottom = jnp.sum(weights, axis=-1, keepdims=True) + jnp.exp(sink - peak)
                    heads.append(dot((weights / bottom).astype(BF16), value))
            win[tp, at, :] = jnp.concatenate(heads, axis=1).astype(BF16)

    def gate(b):
        name = WEIGHTS[10 + b]
        loads[name].wait()

        def step(i, _):
            at = pl.ds(pl.multiple_of(i * 256, LANES), 256)
            gates[b, :, at] = jax.nn.sigmoid(dot(normed[...], w[name][:, at]))
            return 0

        lax.fori_loop(0, block // 256, step, 0)

    def step(k, _):
        @pl.when((z >= k) & (k < n_z))
        def _():
            take_column(k)

        @pl.when(z >= k - 1)
        def _():
            take_rows(k - 1)

        @pl.when(k == 1)
        def _():
            attend(sp, True)
            window()
            start(gather(win, 1))

        @pl.when(k == 2)
        def _():
            gate(0)
            gate(1)

        @pl.when((k > 1) & (z >= k - 1))
        def _():
            c_copy(k - 1, 1 - core).wait_recv()
            attend(column_slot(k - 1), False)

        for d in range(1, n_x):
            @pl.when(z >= k - 1)
            def _():
                d_copy(k - 1, d, 1 - core).wait_recv()

            @pl.when((z >= k - 1) & ((k > 1) | (lax.rem(x + n_x - d, n_x) < x)))
            def _():
                attend(row_slot(k - 1, d), False)

        return 0

    lax.fori_loop(1, max(n_z, 2) + 1, step, 0)

    for h in range(lat_heads):
        lat[tp, :, h * VDIM : (h + 1) * VDIM] = (acc[h] / total[h][:, :1]).astype(BF16)
    start(gather(lat, 2))
    arrived(win, 1)
    for copy in column_local:
        copy.wait()
    for b in range(2):
        for d in range(1, n_tp):
            source = lax.rem(tp + n_tp - d, n_tp)
            ref = columns[b].at[source]
            remote(ref, ref, col_send.at[b, d], col_recv.at[b, d],
                   {"sp": sp, "tp": sibling}).wait_recv()
    window_branch = jnp.zeros((rows, block), F32)
    for j in range(n_tp):
        window_branch = window_branch + dot(win[j], columns[0][j])
    wide_gated = gates[0] * window_branch
    gates[0] = wide_gated
    arrived(lat, 2)
    latent_branch = jnp.zeros((rows, block), F32)
    for j in range(n_tp):
        latent_branch = latent_branch + dot(lat[j], columns[1][j])
    out[...] = (gates[0] + gates[1] * latent_branch).astype(BF16)

    for buf, which in ((feat, 0), (win, 1), (lat, 2)):
        sent(buf, which)
    for copy in column_sends:
        copy.wait_send()

    @pl.when(sp + 1 < n_sp)
    def _():
        halo_copy.wait_send()

    def drain(k, _):
        @pl.when(z >= k)
        def _():
            @pl.when(z + 1 < n_z)
            def _():
                z_copy(k).wait_send()

            for d in range(1, n_x):
                x_copy(k, d).wait_send()
                d_copy(k, d, core).wait_send()

            @pl.when(k > 0)
            def _():
                c_copy(k, core).wait_send()

        return 0

    lax.fori_loop(0, n_z, drain, 0)


def on_device(dims, features, norm_gain, w_query, w_key, w_value, head_sinks, w_query_latent,
              w_kv_latent, w_rope_key, query_latent_gain, kv_latent_gain, w_query_content,
              w_query_rotary, w_key_up, w_value_up, w_branch_window, w_branch_latent,
              w_gate_window, w_gate_latent):
    n_sp, n_tp, n_x = dims
    n_z, n_y = n_sp // n_x, n_tp // 2
    rows, block = features.shape
    width = norm_gain.shape[0]
    latent = w_kv_latent.shape[1]
    lat_heads = w_key_up.shape[1] // NOPE
    positions = lax.axis_index("sp") * rows + jnp.arange(rows, dtype=jnp.int32)
    half_width = ROPE // 2
    frequencies = THETA ** (-jnp.arange(half_width, dtype=F32) / half_width)
    angles = positions.astype(F32)[:, None] * frequencies
    cosine, sine = jnp.cos(angles), jnp.sin(angles)
    cosine = jnp.concatenate([cosine, cosine], axis=1)
    sine = jnp.concatenate([-sine, sine], axis=1)
    weights = (w_kv_latent, w_rope_key, w_key, w_value, w_query, w_query_latent, w_query_content,
               w_query_rotary, w_key_up, w_value_up, w_gate_window, w_gate_latent)
    branches = (w_branch_window, w_branch_latent)
    vmem = pl.BlockSpec(memory_space=pltpu.VMEM)
    hbm = pl.BlockSpec(memory_space=pl.ANY)
    dma = pltpu.SemaphoreType.DMA
    return pl.pallas_call(
        functools.partial(kernel, dims),
        out_shape=jax.ShapeDtypeStruct((rows, block), BF16),
        in_specs=[hbm, vmem, pl.BlockSpec(memory_space=pltpu.SMEM), vmem, vmem, vmem, vmem]
        + [hbm] * (len(weights) + 2),
        out_specs=vmem,
        scratch_shapes=[
            pltpu.VMEM((n_tp, rows, block), BF16),
            pltpu.VMEM((rows, width), BF16),
            pltpu.VMEM((rows, latent), F32),
            *[pltpu.VMEM(weight.shape, BF16) for weight in weights],
            *[pltpu.VMEM((n_tp, branch.shape[0], block), BF16) for branch in branches],
            pltpu.VMEM((n_sp, 2, rows // 2, latent + LANES), BF16),
            pltpu.VMEM((rows, 2 * w_key.shape[1]), BF16),
            pltpu.VMEM((WINDOW, 2 * w_key.shape[1]), BF16),
            pltpu.VMEM((rows, w_query.shape[1]), BF16),
            pltpu.VMEM((lat_heads, rows, NOPE + LANES), BF16),
            pltpu.VMEM((2, rows, block), F32),
            pltpu.VMEM((n_tp, rows, w_query.shape[1]), BF16),
            pltpu.VMEM((n_tp, rows, lat_heads * VDIM), BF16),
            *[pltpu.VMEM((lat_heads, rows, LANES), F32)] * 3,
            dma((len(weights),)),
            dma((1,)),
            dma((2,)),
            dma((2, n_tp)),
            dma((2, n_tp)),
            dma((2,)),
            *[dma((3, n_y))] * 4,
            dma((n_z + 1,)),
            dma((n_z + 1,)),
            dma((n_z, n_x)),
            dma((n_z, n_x)),
            dma((n_z,)),
            dma((n_z,)),
            dma((n_z, n_x)),
            dma((n_z, n_x)),
        ],
        compiler_params=pltpu.CompilerParams(
            collective_id=0, has_side_effects=True, vmem_limit_bytes=60 * 1024 * 1024
        ),
    )(features, norm_gain[None, :], head_sinks[None, :], query_latent_gain[None, :],
      kv_latent_gain[None, :], cosine, sine, *weights, *branches)


def solution(mesh):
    n_sp, n_tp = mesh.shape["sp"], mesh.shape["tp"]
    n_x = 1
    while n_sp % (2 * n_x) == 0 and 8 * n_x * n_x <= n_sp:
        n_x *= 2
    return jax.shard_map(
        functools.partial(on_device, (n_sp, n_tp, n_x)),
        mesh=mesh,
        in_specs=(
            P("sp", "tp"),
            P(),
            P(None, "tp"),
            P(None, "tp"),
            P(None, "tp"),
            P("tp"),
            P(),
            P(),
            P(),
            P(),
            P(),
            P(None, "tp"),
            P(None, "tp"),
            P(None, "tp"),
            P(None, "tp"),
            P("tp", None),
            P("tp", None),
            P(None, "tp"),
            P(None, "tp"),
        ),
        out_specs=P("sp", "tp"),
        check_vma=False,
    )
```

time: 169 us -> 68.1 us (0.40)
  the two profiles are of different devices: /device:TPU:0 before, /device:TPU:27 now
where the time goes in v1:
time: 68.1 us; the launch traced here: 67.9 us
  Pallas kernels  62.5 us (92%)
  local copies, waits for them, and re-layouts  3.71 us (5%)
  other arithmetic  1.71 us (3%)
    pallas_call x1, Pallas kernels, on_device(): pl.pallas_call(functools.partial(kernel, dims), out_shape=jax.ShapeDtypeS...  62.5 us
    unnamed x2, local copies, waits for them, and re-layouts  3.71 us

profile of v1, /device:TPU:27, one launch (start us, length us, event | category | flops | bytes accessed | tf_op | source)
XLA Modules:
  0.0 67.9 jit_solution(11345251299678393010)
XLA Ops:
  0.0 0.8 %fusion = (f32[384,32]{1,0:T(8,128)S(1)}, f32[384,32]{1,0:T(8,128)S(1)}, f32[384,32]{1,0:T(8,128)S(1)}) fusion(f32[32]{0:T(128)S(1)} %multiply_power_fusion, f32[384]{0:T(512)S(1)} %add_convert_fusion), kind=kLoop, calls=%fused_computation.4 | loop fusion | flops 24576 | bytes 149120 | tf_op jit(solution)/shard_map/neg | solution.py:464
  0.8 0.9 %pad_maximum_fusion = (f32[384,64]{1,0:T(8,128)}, f32[384,64]{1,0:T(8,128)}) fusion(f32[384,32]{1,0:T(8,128)S(1)} %get-tuple-element.7, f32[384,32]{1,0:T(8,128)S(1)} %get-tuple-element.6, f32[384,32]{1,0:T(8,128)S(1)} %get-tuple-element.5), kind=kLoop, calls=%fused_computation.2 | loop fusion | flops 49152 | bytes 344064 | tf_op jit(solution)/shard_map/concatenate | solution.py:463
  1.7 1.9 %copy.22.refs_8_ = bf16[2048,64]{1,0:T(8,128)(2,1)} copy(bf16[2048,64]{0,1:T(8,128)(2,1)} %param.27) | data formatting | bytes 524288 | tf_op args[8]
  3.7 62.5 %shard_map.181 = bf16[384,512]{1,0:T(8,128)(2,1)} custom-call(bf16[384,512]{1,0:T(8,128)(2,1)} %refs_0_.1, f32[1,2048]{1,0:T(1,128)} %bitcast.4, f32[1,4]{1,0:T(1,128)} %bitcast.7, f32[1,512]{1,0:T(1,128)} %bitcast.5, f32[1,512]{1,0:T(1,128)} %bitcast.6, f32[384,64]{1,0:T(8,128)} %get-tuple-element.8.refs_5_, f32[384,64]{1,0:T(8,128)} %get-tuple-element.9.refs_6_, ...), custom_call_target="tpu_custom_call" | custom-call | tf_op jit(solution)/shard_map/pallas_call | solution.py:471
  66.1 1.8 %copy.24 = bf16[384,512]{1,0:T(8,128)(2,1)} copy(bf16[384,512]{1,0:T(8,128)(2,1)} %shard_map.181) | data formatting | bytes 786432
  (2 shorter events, 0.0 us)

commit v2 on v1

--- a/solution.py
+++ b/solution.py
@@ -49,7 +49,8 @@
 def kernel(dims, *refs):
     n_sp, n_tp, n_x = dims
     n_z, n_y = n_sp // n_x, n_tp // 2
-    features, norm_gain, sinks, q_gain, kv_gain, cosine, sine = refs[:7]
+    features, norm_gain, sinks, q_gain, kv_gain, frequency = refs[:6]
+    refs = (None,) + refs
     w_hbm = dict(zip(WEIGHTS, refs[7:19]))
     branch_hbm = refs[19:21]
     out = refs[21]
@@ -59,6 +60,7 @@
     kvb, local_kv, halo, queries, q_full, gates, win, lat, top, total, acc = refs[39:50]
     w_sem, own_sem, col_own, col_send, col_recv, halo_sem, y_send, y_recv, s_send, s_recv = refs[50:60]
     z_send, z_recv, x_send, x_recv, c_send, c_recv, d_send, d_recv = refs[60:68]
+    cosine, sine = refs[68:70]
 
     sp, tp = lax.axis_index("sp"), lax.axis_index("tp")
     z, x = sp // n_x, lax.rem(sp, n_x)
@@ -73,8 +75,12 @@
     latent = w_hbm["kv_latent"].shape[1]
 
     loads = {}
-    own_feat = pltpu.make_async_copy(features, feat.at[tp], own_sem.at[0])
-    own_feat.start()
+    own_feat = [
+        pltpu.make_async_copy(features.at[pl.ds(h * half, half)], feat.at[tp, h], own_sem.at[h])
+        for h in range(2)
+    ]
+    for copy in own_feat:
+        copy.start()
     for i, name in enumerate(WEIGHTS):
         loads[name] = pltpu.make_async_copy(w_hbm[name], w[name], w_sem.at[i])
         loads[name].start()
@@ -119,8 +125,8 @@
         + jnp.where(sp + 1 < n_sp, one, none) + jnp.where(sp > 0, one, none),
     )
 
-    def gather(buf, which):
-        own = buf.at[tp]
+    def gather(view, which):
+        own = view(tp)
         sends = [
             remote(own, own, y_send.at[which, d], y_recv.at[which, d],
                    {"sp": sp, "tp": lax.rem(y + d, n_y) * 2 + core})
@@ -134,21 +140,22 @@
         for copy in copies:
             copy.start()
 
-    def arrived(buf, which):
+    def forward(view, which):
         for d in range(1, n_y):
-            slot = lax.rem(y + n_y - d, n_y) * 2 + core
-            ref = buf.at[slot]
+            ref = view(lax.rem(y + n_y - d, n_y) * 2 + core)
             remote(ref, ref, y_send.at[which, d], y_recv.at[which, d],
                    {"sp": sp, "tp": sibling}).wait_recv()
             remote(ref, ref, s_send.at[which, d], s_recv.at[which, d],
                    {"sp": sp, "tp": sibling}).start()
+
+    def arrived(view, which):
         for d in range(n_y):
-            ref = buf.at[lax.rem(y + n_y - d, n_y) * 2 + (1 - core)]
+            ref = view(lax.rem(y + n_y - d, n_y) * 2 + (1 - core))
             remote(ref, ref, s_send.at[which, d], s_recv.at[which, d],
                    {"sp": sp, "tp": sibling}).wait_recv()
 
-    def sent(buf, which):
-        own = buf.at[tp]
+    def sent(view, which):
+        own = view(tp)
         for d in range(1, n_y):
             remote(own, own, y_send.at[which, d], y_recv.at[which, d],
                    {"sp": sp, "tp": sibling}).wait_send()
@@ -156,9 +163,20 @@
             remote(own, own, s_send.at[which, d], s_recv.at[which, d],
                    {"sp": sp, "tp": sibling}).wait_send()
 
-    own_feat.wait()
-    start(gather(feat, 0))
-    arrived(feat, 0)
+    feat_half = [lambda slot, h=h: feat.at[slot, h] for h in range(2)]
+    lat_half = [lambda slot, h=h: lat.at[slot, h] for h in range(2)]
+    win_all = lambda slot: win.at[slot]
+
+    for h in range(2):
+        own_feat[h].wait()
+        start(gather(feat_half[h], h))
+
+    positions = (sp * rows + lax.broadcasted_iota(jnp.int32, (rows, ROPE), 0)).astype(F32)
+    angles = positions * frequency[...]
+    lane = lax.broadcasted_iota(jnp.int32, (rows, ROPE), 1)
+    cosine[...] = jnp.cos(angles)
+    turned = jnp.sin(angles)
+    sine[...] = jnp.where(lane < ROPE // 2, -turned, turned)
 
     def column_copies():
         local, sends = [], []
@@ -176,84 +194,99 @@
         return local, sends
 
     column_local, column_sends = column_copies()
-    start(column_local)
-    start(column_sends)
-
-    squares = jnp.zeros((rows, 1), F32)
-    for j in range(n_tp):
-        piece = feat[j].astype(F32)
-        squares = squares + jnp.sum(piece * piece, axis=-1, keepdims=True)
-    scale = lax.rsqrt(squares / (n_tp * block) + EPS)
-    for j in range(n_tp):
-        span = slice(j * block, (j + 1) * block)
-        normed[:, span] = (feat[j].astype(F32) * scale * norm_gain[:, span]).astype(BF16)
-
-    def wide_dot(name):
-        loads[name].wait()
+
+    def normalize(h):
+        squares = jnp.zeros((half, 1), F32)
+        for j in range(n_tp):
+            piece = feat[j, h].astype(F32)
+            squares = squares + jnp.sum(piece * piece, axis=-1, keepdims=True)
+        scale = lax.rsqrt(squares / (n_tp * block) + EPS)
+        for j in range(n_tp):
+            span = slice(j * block, (j + 1) * block)
+            piece = feat[j, h].astype(F32) * scale * norm_gain[:, span]
+            normed[h * half : (h + 1) * half, span] = piece.astype(BF16)
+
+    def wide_dot(name, at):
         tile = min(256, latent)
 
         def step(i, _):
-            at = pl.ds(pl.multiple_of(i * tile, LANES), tile)
-            wide[:, at] = dot(normed[...], w[name][:, at])
+            to = pl.ds(pl.multiple_of(i * tile, LANES), tile)
+            wide[at, to] = dot(normed[at, :], w[name][:, to])
             return 0
 
         lax.fori_loop(0, w[name].shape[1] // tile, step, 0)
 
-    wide_dot("kv_latent")
-    latents = rms_rows(wide[...], kv_gain[...]).astype(BF16)
-    loads["rope"].wait()
-    rope = dot(normed[...], w["rope"][...])
-    rope = rope * cosine[...] + swap_halves(rope) * sine[...]
     padding = jnp.zeros((rows, LANES - ROPE), F32)
-    rope = jnp.concatenate([rope, padding], axis=1).astype(BF16)
-    kvb[sp, :, :, :latent] = latents.reshape(2, half, latent)
-    kvb[sp, :, :, latent:] = rope.reshape(2, half, LANES)
+
+    def latents(h):
+        at = slice(h * half, (h + 1) * half)
+        wide_dot("kv_latent", at)
+        rope = dot_t(normed[at, :], w["rope"][...])
+        rope = rope * cosine[at, :] + swap_halves(rope) * sine[at, :]
+        rope = jnp.concatenate([rope, padding[at]], axis=1).astype(BF16)
+        kvb[sp, h, :, :, :latent] = (
+            rms_rows(wide[at, :], kv_gain[...]).astype(BF16).reshape(2, half // 2, latent))
+        kvb[sp, h, :, :, latent:] = rope.reshape(2, half // 2, LANES)
 
     def column_slot(k):
         return (z - k) * n_x + x
 
-    def z_copy(k):
-        ref = kvb.at[column_slot(k), core]
-        return remote(ref, ref, z_send.at[k], z_recv.at[k + 1], {"sp": sp + n_x, "tp": tp})
-
-    def x_copy(k, d):
-        ref = kvb.at[column_slot(k), core]
-        return remote(ref, ref, x_send.at[k, d], x_recv.at[k, d],
-                      {"sp": z * n_x + lax.rem(x + d, n_x), "tp": tp})
-
-    def c_copy(k, which):
-        ref = kvb.at[column_slot(k), which]
-        return remote(ref, ref, c_send.at[k], c_recv.at[k], {"sp": sp, "tp": sibling})
-
     def row_slot(k, d):
         return (z - k) * n_x + lax.rem(x + n_x - d, n_x)
 
-    def d_copy(k, d, which):
-        ref = kvb.at[row_slot(k, d), which]
-        return remote(ref, ref, d_send.at[k, d], d_recv.at[k, d], {"sp": sp, "tp": sibling})
-
-    def pass_on(k):
+    def z_copy(k, h):
+        ref = kvb.at[column_slot(k), h, core]
+        return remote(ref, ref, z_send.at[h, k], z_recv.at[h, k + 1], {"sp": sp + n_x, "tp": tp})
+
+    def x_copy(k, d, h):
+        ref = kvb.at[column_slot(k), h, core]
+        return remote(ref, ref, x_send.at[h, k, d], x_recv.at[h, k, d],
+                      {"sp": z * n_x + lax.rem(x + d, n_x), "tp": tp})
+
+    def c_copy(k, h, which):
+        ref = kvb.at[column_slot(k), h, which]
+        return remote(ref, ref, c_send.at[h, k], c_recv.at[h, k], {"sp": sp, "tp": sibling})
+
+    def d_copy(k, d, h, which):
+        ref = kvb.at[row_slot(k, d), h, which]
+        return remote(ref, ref, d_send.at[h, k, d], d_recv.at[h, k, d],
+                      {"sp": sp, "tp": sibling})
+
+    def pass_on(k, h):
         @pl.when(z + 1 < n_z)
         def _():
-            z_copy(k).start()
+            z_copy(k, h).start()
 
         for d in range(1, n_x):
-            x_copy(k, d).start()
+            x_copy(k, d, h).start()
 
     def take_column(k):
-        ref = kvb.at[column_slot(k), core]
-        remote(ref, ref, z_send.at[k], z_recv.at[k], {"sp": sp, "tp": sibling}).wait_recv()
-        pass_on(k)
-        c_copy(k, core).start()
+        for h in range(2):
+            ref = kvb.at[column_slot(k), h, core]
+            remote(ref, ref, z_send.at[h, k], z_recv.at[h, k],
+                   {"sp": sp, "tp": sibling}).wait_recv()
+            pass_on(k, h)
+            c_copy(k, h, core).start()
 
     def take_rows(k):
-        for d in range(1, n_x):
-            ref = kvb.at[row_slot(k, d), core]
-            remote(ref, ref, x_send.at[k, d], x_recv.at[k, d],
-                   {"sp": sp, "tp": sibling}).wait_recv()
-            d_copy(k, d, core).start()
-
-    pass_on(0)
+        for h in range(2):
+            for d in range(1, n_x):
+                ref = kvb.at[row_slot(k, d), h, core]
+                remote(ref, ref, x_send.at[h, k, d], x_recv.at[h, k, d],
+                       {"sp": sp, "tp": sibling}).wait_recv()
+                d_copy(k, d, h, core).start()
+
+    loads["kv_latent"].wait()
+    loads["rope"].wait()
+    for h in range(2):
+        forward(feat_half[h], h)
+        arrived(feat_half[h], h)
+        if h == 1:
+            start(column_local)
+            start(column_sends)
+        normalize(h)
+        latents(h)
+        pass_on(0, h)
 
     loads["key"].wait()
     loads["value"].wait()
@@ -269,7 +302,8 @@
     loads["query"].wait()
     queries[...] = dot(normed[...], w["query"][...]).astype(BF16)
 
-    wide_dot("query_latent")
+    loads["query_latent"].wait()
+    wide_dot("query_latent", slice(0, rows))
     latent_query = rms_rows(wide[...], q_gain[...]).astype(BF16)
     loads["content"].wait()
     loads["rotary"].wait()
@@ -360,30 +394,35 @@
         def _():
             take_column(k)
 
-        @pl.when(z >= k - 1)
-        def _():
-            take_rows(k - 1)
-
         @pl.when(k == 1)
         def _():
             attend(sp, True)
+
+        @pl.when(k == 2)
+        def _():
             window()
-            start(gather(win, 1))
-
-        @pl.when(k == 2)
+            start(gather(win_all, 2))
+
+        @pl.when(k == 3)
         def _():
             gate(0)
             gate(1)
 
         @pl.when((k > 1) & (z >= k - 1))
         def _():
-            c_copy(k - 1, 1 - core).wait_recv()
+            for h in range(2):
+                c_copy(k - 1, h, 1 - core).wait_recv()
             attend(column_slot(k - 1), False)
+
+        @pl.when(z >= k - 1)
+        def _():
+            take_rows(k - 1)
 
         for d in range(1, n_x):
             @pl.when(z >= k - 1)
             def _():
-                d_copy(k - 1, d, 1 - core).wait_recv()
+                for h in range(2):
+                    d_copy(k - 1, d, h, 1 - core).wait_recv()
 
             @pl.when((z >= k - 1) & ((k > 1) | (lax.rem(x + n_x - d, n_x) < x)))
             def _():
@@ -391,12 +430,16 @@
 
         return 0
 
-    lax.fori_loop(1, max(n_z, 2) + 1, step, 0)
-
-    for h in range(lat_heads):
-        lat[tp, :, h * VDIM : (h + 1) * VDIM] = (acc[h] / total[h][:, :1]).astype(BF16)
-    start(gather(lat, 2))
-    arrived(win, 1)
+    lax.fori_loop(1, max(n_z, 3) + 1, step, 0)
+
+    for part in range(2):
+        at = slice(part * half, (part + 1) * half)
+        for h in range(lat_heads):
+            lat[tp, part, :, h * VDIM : (h + 1) * VDIM] = (
+                acc[h, at] / total[h, at][:, :1]).astype(BF16)
+        start(gather(lat_half[part], 3 + part))
+    forward(win_all, 2)
+    arrived(win_all, 2)
     for copy in column_local:
         copy.wait()
     for b in range(2):
@@ -408,16 +451,18 @@
     window_branch = jnp.zeros((rows, block), F32)
     for j in range(n_tp):
         window_branch = window_branch + dot(win[j], columns[0][j])
-    wide_gated = gates[0] * window_branch
-    gates[0] = wide_gated
-    arrived(lat, 2)
-    latent_branch = jnp.zeros((rows, block), F32)
-    for j in range(n_tp):
-        latent_branch = latent_branch + dot(lat[j], columns[1][j])
-    out[...] = (gates[0] + gates[1] * latent_branch).astype(BF16)
-
-    for buf, which in ((feat, 0), (win, 1), (lat, 2)):
-        sent(buf, which)
+    gates[0] = gates[0] * window_branch
+    for part in range(2):
+        at = slice(part * half, (part + 1) * half)
+        forward(lat_half[part], 3 + part)
+        arrived(lat_half[part], 3 + part)
+        latent_branch = jnp.zeros((half, block), F32)
+        for j in range(n_tp):
+            latent_branch = latent_branch + dot(lat[j, part], columns[1][j])
+        out[at, :] = (gates[0, at] + gates[1, at] * latent_branch).astype(BF16)
+
+    for which, view in enumerate((*feat_half, win_all, *lat_half)):
+        sent(view, which)
     for copy in column_sends:
         copy.wait_send()
 
@@ -428,17 +473,18 @@
     def drain(k, _):
         @pl.when(z >= k)
         def _():
-            @pl.when(z + 1 < n_z)
-            def _():
-                z_copy(k).wait_send()
-
-            for d in range(1, n_x):
-                x_copy(k, d).wait_send()
-                d_copy(k, d, core).wait_send()
-
-            @pl.when(k > 0)
-            def _():
-                c_copy(k, core).wait_send()
+            for h in range(2):
+                @pl.when(z + 1 < n_z)
+                def _():
+                    z_copy(k, h).wait_send()
+
+                for d in range(1, n_x):
+                    x_copy(k, d, h).wait_send()
+                    d_copy(k, d, h, core).wait_send()
+
+                @pl.when(k > 0)
+                def _():
+                    c_copy(k, h, core).wait_send()
 
         return 0
 
@@ -455,14 +501,10 @@
     width = norm_gain.shape[0]
     latent = w_kv_latent.shape[1]
     lat_heads = w_key_up.shape[1] // NOPE
-    positions = lax.axis_index("sp") * rows + jnp.arange(rows, dtype=jnp.int32)
     half_width = ROPE // 2
-    frequencies = THETA ** (-jnp.arange(half_width, dtype=F32) / half_width)
-    angles = positions.astype(F32)[:, None] * frequencies
-    cosine, sine = jnp.cos(angles), jnp.sin(angles)
-    cosine = jnp.concatenate([cosine, cosine], axis=1)
-    sine = jnp.concatenate([-sine, sine], axis=1)
-    weights = (w_kv_latent, w_rope_key, w_key, w_value, w_query, w_query_latent, w_query_content,
+    entry = lax.rem(jnp.arange(ROPE, dtype=jnp.int32), half_width).astype(F32)
+    frequency = (THETA ** (-entry / half_width))[None, :]
+    weights = (w_kv_latent, w_rope_key.T, w_key, w_value, w_query, w_query_latent, w_query_content,
                w_query_rotary, w_key_up, w_value_up, w_gate_window, w_gate_latent)
     branches = (w_branch_window, w_branch_latent)
     vmem = pl.BlockSpec(memory_space=pltpu.VMEM)
@@ -471,45 +513,46 @@
     return pl.pallas_call(
         functools.partial(kernel, dims),
         out_shape=jax.ShapeDtypeStruct((rows, block), BF16),
-        in_specs=[hbm, vmem, pl.BlockSpec(memory_space=pltpu.SMEM), vmem, vmem, vmem, vmem]
+        in_specs=[hbm, vmem, pl.BlockSpec(memory_space=pltpu.SMEM), vmem, vmem, vmem]
         + [hbm] * (len(weights) + 2),
         out_specs=vmem,
         scratch_shapes=[
-            pltpu.VMEM((n_tp, rows, block), BF16),
+            pltpu.VMEM((n_tp, 2, rows // 2, block), BF16),
             pltpu.VMEM((rows, width), BF16),
             pltpu.VMEM((rows, latent), F32),
             *[pltpu.VMEM(weight.shape, BF16) for weight in weights],
             *[pltpu.VMEM((n_tp, branch.shape[0], block), BF16) for branch in branches],
-            pltpu.VMEM((n_sp, 2, rows // 2, latent + LANES), BF16),
+            pltpu.VMEM((n_sp, 2, 2, rows // 4, latent + LANES), BF16),
             pltpu.VMEM((rows, 2 * w_key.shape[1]), BF16),
             pltpu.VMEM((WINDOW, 2 * w_key.shape[1]), BF16),
             pltpu.VMEM((rows, w_query.shape[1]), BF16),
             pltpu.VMEM((lat_heads, rows, NOPE + LANES), BF16),
             pltpu.VMEM((2, rows, block), F32),
             pltpu.VMEM((n_tp, rows, w_query.shape[1]), BF16),
-            pltpu.VMEM((n_tp, rows, lat_heads * VDIM), BF16),
+            pltpu.VMEM((n_tp, 2, rows // 2, lat_heads * VDIM), BF16),
             *[pltpu.VMEM((lat_heads, rows, LANES), F32)] * 3,
             dma((len(weights),)),
-            dma((1,)),
+            dma((2,)),
             dma((2,)),
             dma((2, n_tp)),
             dma((2, n_tp)),
             dma((2,)),
-            *[dma((3, n_y))] * 4,
-            dma((n_z + 1,)),
-            dma((n_z + 1,)),
-            dma((n_z, n_x)),
-            dma((n_z, n_x)),
-            dma((n_z,)),
-            dma((n_z,)),
-            dma((n_z, n_x)),
-            dma((n_z, n_x)),
+            *[dma((5, n_y))] * 4,
+            dma((2, n_z + 1)),
+            dma((2, n_z + 1)),
+            dma((2, n_z, n_x)),
+            dma((2, n_z, n_x)),
+            dma((2, n_z)),
+            dma((2, n_z)),
+            dma((2, n_z, n_x)),
+            dma((2, n_z, n_x)),
+            *[pltpu.VMEM((rows, ROPE), F32)] * 2,
         ],
         compiler_params=pltpu.CompilerParams(
             collective_id=0, has_side_effects=True, vmem_limit_bytes=60 * 1024 * 1024
         ),
     )(features, norm_gain[None, :], head_sinks[None, :], query_latent_gain[None, :],
-      kv_latent_gain[None, :], cosine, sine, *weights, *branches)
+      kv_latent_gain[None, :], frequency, *weights, *branches)
 
 
 def solution(mesh):

time: 68.1 us -> 62.7 us (0.921)
  Pallas kernels: 62.5 us -> 60.2 us
  local copies, waits for them, and re-layouts: 3.71 us -> 1.77 us
  other arithmetic: 1.71 us -> 0.52 us
    pallas_call x1, Pallas kernels: 62.5 us -> 60.2 us  [on_device(): pl.pallas_call(functools.partial(kernel, dims), out_shape=jax.ShapeDtypeS...]
    unnamed x2 -> x1, local copies, waits for them, and re-layouts: 3.71 us -> 1.77 us
    concatenate x1 -> x0, other arithmetic: 0.92 us -> none  [on_device(): cosine = jnp.concatenate([cosine, cosine], axis=1)]
    neg x1 -> x0, other arithmetic: 0.77 us -> none  [on_device(): sine = jnp.concatenate([-sine, sine], axis=1)]
where the time goes in v2:
time: 62.7 us; the launch traced here: 62.5 us
  Pallas kernels  60.2 us (96%)
  local copies, waits for them, and re-layouts  1.77 us (3%)
    pallas_call x1, Pallas kernels, on_device(): pl.pallas_call(functools.partial(kernel, dims), out_shape=jax.ShapeDtypeS...  60.2 us
    unnamed x1, local copies, waits for them, and re-layouts  1.77 us

profile of v2, /device:TPU:27, one launch (start us, length us, event | category | flops | bytes accessed | tf_op | source)
XLA Modules:
  0.0 62.5 jit_solution(12137461544915212641)
XLA Ops:
  0.0 0.5 multiply_power_fusion.refs_5_
  0.5 60.2 %shard_map.181 = bf16[384,512]{1,0:T(8,128)(2,1)} custom-call(bf16[384,512]{1,0:T(8,128)(2,1)} %refs_0_.1, f32[1,2048]{1,0:T(1,128)} %bitcast.6, f32[1,4]{1,0:T(1,128)} %bitcast.9, f32[1,512]{1,0:T(1,128)} %bitcast.7, f32[1,512]{1,0:T(1,128)} %bitcast.8, f32[1,64]{1,0:T(1,128)} %multiply_power_fusion.refs_5_, bf16[2048,512]{1,0:T(8,128)(2,1)} %refs_6_.1, ...), custom_call_target="tpu_custom_call" | custom-call | tf_op jit(solution)/shard_map/pallas_call | solution.py:513
  60.7 1.8 %copy.21 = bf16[384,512]{1,0:T(8,128)(2,1)} copy(bf16[384,512]{1,0:T(8,128)(2,1)} %shard_map.181) | data formatting | bytes 786432

commit v3 on v2

--- a/solution.py
+++ b/solution.py
@@ -18,6 +18,7 @@
 THETA = 10000.0
 NEGATIVE = -1e30
 LANES = 128
+LOG2_E = 1.4426950408889634
 MESH = pl.DeviceIdType.MESH
 BF16 = jnp.bfloat16
 F32 = jnp.float32
@@ -324,7 +325,7 @@
         values = dot(source, w["value_up"][...]).astype(BF16)
         for h in range(lat_heads):
             key = jnp.concatenate([keys[:, h * NOPE : (h + 1) * NOPE], rope_part], axis=1)
-            scores = dot_t(q_full[h], key) * (NOPE + ROPE) ** (-0.5)
+            scores = dot_t(q_full[h], key) * ((NOPE + ROPE) ** (-0.5) * LOG2_E)
             if diagonal:
                 live = (lax.broadcasted_iota(jnp.int32, scores.shape, 1)
                         <= lax.broadcasted_iota(jnp.int32, scores.shape, 0))
@@ -333,8 +334,8 @@
             if not diagonal:
                 before = top[h][:, :1]
                 peak = jnp.maximum(peak, before)
-                fade = jnp.exp(before - peak)
-            weights = jnp.exp(scores - peak)
+                fade = jnp.exp2(before - peak)
+            weights = jnp.exp2(scores - peak)
             weight_sum = jnp.sum(weights, axis=-1, keepdims=True)
             part = dot(weights.astype(BF16), values[:, h * VDIM : (h + 1) * VDIM])
             if not diagonal:
@@ -403,11 +404,6 @@
             window()
             start(gather(win_all, 2))
 
-        @pl.when(k == 3)
-        def _():
-            gate(0)
-            gate(1)
-
         @pl.when((k > 1) & (z >= k - 1))
         def _():
             for h in range(2):
@@ -430,7 +426,7 @@
 
         return 0
 
-    lax.fori_loop(1, max(n_z, 3) + 1, step, 0)
+    lax.fori_loop(1, max(n_z, 2) + 1, step, 0)
 
     for part in range(2):
         at = slice(part * half, (part + 1) * half)
@@ -438,7 +434,9 @@
             lat[tp, part, :, h * VDIM : (h + 1) * VDIM] = (
                 acc[h, at] / total[h, at][:, :1]).astype(BF16)
         start(gather(lat_half[part], 3 + part))
+    gate(0)
     forward(win_all, 2)
+    gate(1)
     arrived(win_all, 2)
     for copy in column_local:
         copy.wait()

time: 62.7 us -> 60.3 us (0.962)
  Pallas kernels: 60.2 us -> 57.8 us
    pallas_call x1, Pallas kernels: 60.2 us -> 57.8 us  [on_device(): pl.pallas_call(functools.partial(kernel, dims), out_shape=jax.ShapeDtypeS...]
where the time goes in v3:
time: 60.3 us; the launch traced here: 60.1 us
  Pallas kernels  57.8 us (96%)
  local copies, waits for them, and re-layouts  1.77 us (3%)
    pallas_call x1, Pallas kernels, on_device(): pl.pallas_call(functools.partial(kernel, dims), out_shape=jax.ShapeDtypeS...  57.8 us
    unnamed x1, local copies, waits for them, and re-layouts  1.77 us

profile of v3, /device:TPU:27, one launch (start us, length us, event | category | flops | bytes accessed | tf_op | source)
XLA Modules:
  0.0 60.1 jit_solution(4052148196184801607)
XLA Ops:
  0.0 0.5 multiply_power_fusion.refs_5_
  0.5 57.8 %shard_map.181 = bf16[384,512]{1,0:T(8,128)(2,1)} custom-call(bf16[384,512]{1,0:T(8,128)(2,1)} %refs_0_.1, f32[1,2048]{1,0:T(1,128)} %bitcast.6, f32[1,4]{1,0:T(1,128)} %bitcast.9, f32[1,512]{1,0:T(1,128)} %bitcast.7, f32[1,512]{1,0:T(1,128)} %bitcast.8, f32[1,64]{1,0:T(1,128)} %multiply_power_fusion.refs_5_, bf16[2048,512]{1,0:T(8,128)(2,1)} %refs_6_.1, ...), custom_call_target="tpu_custom_call" | custom-call | tf_op jit(solution)/shard_map/pallas_call | solution.py:511
  58.3 1.8 %copy.21 = bf16[384,512]{1,0:T(8,128)(2,1)} copy(bf16[384,512]{1,0:T(8,128)(2,1)} %shard_map.181) | data formatting | bytes 786432
